TPU v7x, 32 devices: a whole 2x2x4 slice. The times are simulated.
32 devices in a mesh: rep: 2 (over x), fs: 8 (over z, y), tp: 2 (over core).
Axes of the slice: x: 2, y: 2, z: 4, core: 2. Of those that a mesh axis runs over, the one named last changes fastest.
Arguments:
- tokens: bfloat16 [5120, 2048], P(('rep', 'fs')), may hold values from -6 to 6
- mixer_out: bfloat16 [5120, 2048], P(('rep', 'fs')), may hold values from -6 to 6
- gate_first: bfloat16 [2048, 2816], P('fs', 'tp'), may hold values from -0.125 to 0.125
- up_first: bfloat16 [2048, 2816], P('fs', 'tp'), may hold values from -0.125 to 0.125
- down_first: bfloat16 [2816, 2048], P('tp', 'fs'), may hold values from -0.3125 to 0.3125
- gate_second: bfloat16 [2048, 2816], P('fs', 'tp'), may hold values from -0.125 to 0.125
- up_second: bfloat16 [2048, 2816], P('fs', 'tp'), may hold values from -0.125 to 0.125
- down_second: bfloat16 [2816, 2048], P('tp', 'fs'), may hold values from -0.3125 to 0.3125
- gain_first: float32 [2048], replicated, may hold values from 0.1 to 1.9
- bias_first: float32 [2048], replicated, may hold values from -1.5 to 1.5
- gain_middle: float32 [2048], replicated, may hold values from 0.1 to 1.9
- bias_middle: float32 [2048], replicated, may hold values from -1.5 to 1.5
- gain_last: float32 [2048], replicated, may hold values from 0.1 to 1.9
- bias_last: float32 [2048], replicated, may hold values from -1.5 to 1.5
Outputs:
- layer_out: bfloat16 [5120, 2048], P(('rep', 'fs'))
All inputs are finite; a program needn't handle non-finite values.
Results may differ from a plain program's by a relative error of at most 0.014.
Values may be sent and summed in bfloat16 or wider, within the bound.
A program may use at most 64 MiB of HBM per device.

v0:
```python
import math
import jax
import jax.numpy as jnp
from jax import lax
from jax.sharding import PartitionSpec as P

residual_scale = math.sqrt(2.0)
norm_eps = 1e-05


def normalize(summed, scaling, offset):
    center = summed - jnp.mean(summed, axis=-1, keepdims=True)
    spread = jnp.mean(center * center, axis=-1, keepdims=True)
    return center * lax.rsqrt(spread + norm_eps) * scaling + offset


def add_columns(inputs, portion):
    return jnp.dot(inputs, portion, preferred_element_type=jnp.float32)


def project_in(inputs, gate_weight, up_weight):
    return (
        add_columns(inputs, lax.all_gather(gate_weight, "fs", axis=0, tiled=True)),
        add_columns(inputs, lax.all_gather(up_weight, "fs", axis=0, tiled=True)),
    )


def project_out(hidden, down_weight):
    return jnp.dot(
        hidden,
        lax.all_gather(down_weight, "fs", axis=1, tiled=True),
        preferred_element_type=jnp.float32,
    )


def half_step(inputs, gate_weight, up_weight, down_weight):
    gate, value = project_in(inputs, gate_weight, up_weight)
    hidden = (jax.nn.silu(gate) * value).astype(jnp.bfloat16)
    partials = project_out(hidden, down_weight)
    summed = lax.psum(partials.astype(jnp.bfloat16), "tp")
    return summed


def per_device(
    tokens,
    mixer_out,
    gate_first,
    up_first,
    down_first,
    gate_second,
    up_second,
    down_second,
    gain_first,
    bias_first,
    gain_middle,
    bias_middle,
    gain_last,
    bias_last,
):
    first_branch = half_step(tokens, gate_first, up_first, down_first)
    first_norm = normalize(
        residual_scale * tokens.astype(jnp.float32) + 0.5 * first_branch.astype(jnp.float32),
        gain_first,
        bias_first,
    ).astype(jnp.bfloat16)
    middle_norm = normalize(
        residual_scale * first_norm.astype(jnp.float32) + mixer_out.astype(jnp.float32),
        gain_middle,
        bias_middle,
    ).astype(jnp.bfloat16)
    second_branch = half_step(middle_norm, gate_second, up_second, down_second)
    finished = normalize(
        residual_scale * middle_norm.astype(jnp.float32) + 0.5 * second_branch.astype(jnp.float32),
        gain_last,
        bias_last,
    ).astype(jnp.bfloat16)
    return finished


def solution(mesh):
    return jax.shard_map(
        per_device,
        mesh=mesh,
        in_specs=(
            P(("rep", "fs"), None),
            P(("rep", "fs"), None),
            P("fs", "tp"),
            P("fs", "tp"),
            P("tp", "fs"),
            P("fs", "tp"),
            P("fs", "tp"),
            P("tp", "fs"),
            P(),
            P(),
            P(),
            P(),
            P(),
            P(),
        ),
        out_specs=P(("rep", "fs"), None),
        check_vma=False,
    )
```

profile of v0, /device:TPU:0, one launch (start us, length us, event | category | flops | bytes accessed | tf_op | source)
XLA Modules:
  0.0 639.6 jit_solution(13720102844049315975)
XLA Ops:
  6.5 0.0 all-gather.7.cloned.1.call-start
  6.5 0.7 all-gather.7.cloned.1.call-update
  7.3 0.0 all-gather.11.cloned.1.call-start
  7.3 0.7 all-gather.11.cloned.1.call-update
  8.0 0.0 all-gather.9.cloned.1.call-start
  8.1 0.7 all-gather.9.cloned.1.call-update
  8.7 0.0 copy-start.2
  8.8 0.0 all-reduce.3.cloned.1.call-start
  8.8 95.8 %all-gather.7.cloned.1.call-done = bf16[2048,1408]{1,0:T(8,128)(2,1)} async-done(((bf16[256,1408]{1,0:T(8,128)(2,1)}), bf16[2048,1408]{1,0:T(8,128)(2,1)}) %all-gather.7.cloned.1.call-update) | async-done | bytes 5767184 | tf_op jit(solution)/shard_map/all_gather | solution.py:23
  104.6 5.2 fusion.7
  109.8 88.2 %all-gather.11.cloned.1.call-done = bf16[1408,2048]{1,0:T(8,128)(2,1)} async-done(((bf16[1408,256]{1,0:T(8,128)(2,1)}), bf16[1408,2048]{1,0:T(8,128)(2,1)}) %all-gather.11.cloned.1.call-update) | async-done | bytes 5767184 | tf_op jit(solution)/shard_map/all_gather | solution.py:31
  198.0 92.7 %all-gather.9.cloned.1.call-done = bf16[2048,1408]{1,0:T(8,128)(2,1)} async-done(((bf16[256,1408]{1,0:T(8,128)(2,1)}), bf16[2048,1408]{1,0:T(8,128)(2,1)}) %all-gather.9.cloned.1.call-update) | async-done | bytes 5767184 | tf_op jit(solution)/shard_map/all_gather | solution.py:24
  290.7 0.0 copy-done.2
  290.7 9.7 %convolution_convert_fusion.1 = bf16[320,2048]{1,0:T(8,128)(2,1)} fusion(bf16[1408,2048]{1,0:T(8,128)(2,1)} %all-gather.11.cloned.1.call-done, bf16[320,2048]{1,0:T(8,128)(2,1)S(1)} %copy-done.2, bf16[2048,1408]{1,0:T(8,128)(2,1)} %all-gather.9.cloned.1.call-done, f32[320,1408]{1,0:T(8,128)S(1)} %fusion.7), kind=kOutput, calls=%fused_computation.3 | convolution fusion | flops 3694346240 | bytes 15958016 | tf_op jit(solution)/shard_map/dot_general | solution.py:29
  300.3 0.0 all-reduce.3.cloned.1.call-update
  300.4 0.0 all-gather.13.cloned.1.call-start
  300.4 0.5 all-gather.13.cloned.1.call-update
  301.0 0.0 all-gather.15.cloned.1.call-start
  301.0 0.5 all-gather.15.cloned.1.call-update
  301.5 0.0 all-gather.17.cloned.1.call-start
  301.6 0.0 copy-start.4
  301.6 0.0 copy-start.5
  301.6 0.7 all-gather.17.cloned.1.call-update
  302.3 0.0 copy-start.1
  302.3 0.2 all-reduce.5.cloned.1.call-start
  302.5 16.1 %all-reduce.3.cloned.1.call-done = bf16[320,2048]{1,0:T(8,128)(2,1)} async-done(((bf16[320,2048]{1,0:T(8,128)(2,1)}), bf16[320,2048]{1,0:T(8,128)(2,1)}) %all-reduce.3.cloned.1.call-update) | async-done | bytes 1310736 | tf_op jit(solution)/shard_map/psum | solution.py:40
  318.6 0.0 copy-start.3
  318.6 2.0 fusion.3
  320.6 0.0 copy-done.3
  320.6 0.8 multiply_reduce_fusion.2
  321.4 0.0 copy-done.4
  321.4 0.0 copy-done.5
  321.5 0.0 copy-done.1
  321.5 1.3 fusion.2
  322.8 0.0 copy-start.6
  322.8 0.0 copy-start.7
  322.8 0.7 multiply_reduce_fusion.1
  323.5 0.0 copy-done.6
  323.5 0.0 copy-done.7
  323.5 0.8 add_convert_fusion.1
  324.3 89.9 %all-gather.13.cloned.1.call-done = bf16[2048,1408]{1,0:T(8,128)(2,1)} async-done(((bf16[256,1408]{1,0:T(8,128)(2,1)}), bf16[2048,1408]{1,0:T(8,128)(2,1)}) %all-gather.13.cloned.1.call-update) | async-done | bytes 5767184 | tf_op jit(solution)/shard_map/all_gather | solution.py:23
  414.2 4.8 fusion.8
  419.0 87.7 %all-gather.15.cloned.1.call-done = bf16[2048,1408]{1,0:T(8,128)(2,1)} async-done(((bf16[256,1408]{1,0:T(8,128)(2,1)}), bf16[2048,1408]{1,0:T(8,128)(2,1)}) %all-gather.15.cloned.1.call-update) | async-done | bytes 5767184 | tf_op jit(solution)/shard_map/all_gather | solution.py:24
  506.7 93.4 %all-gather.17.cloned.1.call-done = bf16[1408,2048]{1,0:T(8,128)(2,1)} async-done(((bf16[1408,256]{1,0:T(8,128)(2,1)}), bf16[1408,2048]{1,0:T(8,128)(2,1)}) %all-gather.17.cloned.1.call-update) | async-done | bytes 5767184 | tf_op jit(solution)/shard_map/all_gather | solution.py:31
  600.1 9.7 %convolution_convert_fusion = bf16[320,2048]{1,0:T(8,128)(2,1)} fusion(bf16[1408,2048]{1,0:T(8,128)(2,1)} %all-gather.17.cloned.1.call-done, bf16[320,2048]{1,0:T(8,128)(2,1)S(1)} %add_convert_fusion.1, bf16[2048,1408]{1,0:T(8,128)(2,1)} %all-gather.15.cloned.1.call-done, f32[320,1408]{1,0:T(8,128)S(1)} %fusion.8), kind=kOutput, calls=%fused_computation.2 | convolution fusion | flops 3694346240 | bytes 15958016 | tf_op jit(solution)/shard_map/dot_general | solution.py:29
  609.8 0.0 all-reduce.5.cloned.1.call-update
  609.8 0.0 copy-start.8
  609.8 0.0 copy-start.9
  609.8 18.2 %all-reduce.5.cloned.1.call-done = bf16[320,2048]{1,0:T(8,128)(2,1)} async-done(((bf16[320,2048]{1,0:T(8,128)(2,1)}), bf16[320,2048]{1,0:T(8,128)(2,1)}) %all-reduce.5.cloned.1.call-update) | async-done | bytes 1310736 | tf_op jit(solution)/shard_map/psum | solution.py:40
  628.0 0.0 copy-start
  628.0 2.0 fusion.4
  630.0 0.0 copy-done
  630.0 0.8 multiply_reduce_fusion
  630.8 0.0 copy-done.8
  630.8 0.0 copy-done.9
  630.9 1.9 add_convert_fusion
  (6 shorter events, 0.0 us)
Async XLA Ops:
  6.5 98.0 %all-gather.7.cloned.1.call-start = ((), (), s32[]{:S(2)}) async-start(), calls=%async_computation | async-start | bytes 6488064 | tf_op jit(solution)/shard_map/all_gather | solution.py:23
  7.3 190.7 %all-gather.11.cloned.1.call-start = ((), (), s32[]{:S(2)}) async-start(), calls=%async_computation.2 | async-start | bytes 6488064 | tf_op jit(solution)/shard_map/all_gather | solution.py:31
  8.0 282.7 %all-gather.9.cloned.1.call-start = ((), (), s32[]{:S(2)}) async-start(), calls=%async_computation.1 | async-start | bytes 6488064 | tf_op jit(solution)/shard_map/all_gather | solution.py:24
  8.7 281.9 %copy-start.2 = (bf16[320,2048]{1,0:T(8,128)(2,1)S(1)}, bf16[320,2048]{1,0:T(8,128)(2,1)}, u32[]{:S(2)}) copy-start(bf16[320,2048]{1,0:T(8,128)(2,1)} %param.14) | copy-start | bytes 3932164
  8.8 309.8 %all-reduce.3.cloned.1.call-start = ((), (), s32[]{:S(2)}) async-start(), calls=%async_computation.3 | async-start | bytes 2621440 | tf_op jit(solution)/shard_map/psum | solution.py:40
  300.4 113.8 %all-gather.13.cloned.1.call-start = ((), (), s32[]{:S(2)}) async-start(), calls=%async_computation.4 | async-start | bytes 6488064 | tf_op jit(solution)/shard_map/all_gather | solution.py:23
  301.0 205.8 %all-gather.15.cloned.1.call-start = ((), (), s32[]{:S(2)}) async-start(), calls=%async_computation.5 | async-start | bytes 6488064 | tf_op jit(solution)/shard_map/all_gather | solution.py:24
  301.5 298.6 %all-gather.17.cloned.1.call-start = ((), (), s32[]{:S(2)}) async-start(), calls=%async_computation.6 | async-start | bytes 6488064 | tf_op jit(solution)/shard_map/all_gather | solution.py:31
  301.6 19.9 %copy-start.4 = (f32[2048]{0:T(1024)S(1)}, f32[2048]{0:T(1024)}, u32[]{:S(2)}) copy-start(f32[2048]{0:T(1024)} %param.23) | copy-start | bytes 24580
  301.6 19.9 %copy-start.5 = (f32[2048]{0:T(1024)S(1)}, f32[2048]{0:T(1024)}, u32[]{:S(2)}) copy-start(f32[2048]{0:T(1024)} %param.22) | copy-start | bytes 24580
  302.3 19.2 %copy-start.1 = (bf16[320,2048]{1,0:T(8,128)(2,1)S(1)}, bf16[320,2048]{1,0:T(8,128)(2,1)}, u32[]{:S(2)}) copy-start(bf16[320,2048]{1,0:T(8,128)(2,1)} %param.15) | copy-start | bytes 3932164
  302.3 325.7 %all-reduce.5.cloned.1.call-start = ((), (), s32[]{:S(2)}) async-start(), calls=%async_computation.7 | async-start | bytes 2621440 | tf_op jit(solution)/shard_map/psum | solution.py:40
  318.6 2.0 copy-start.3
  322.8 0.7 copy-start.6
  322.8 0.7 copy-start.7
  609.8 21.0 %copy-start.8 = (f32[2048]{0:T(1024)S(1)}, f32[2048]{0:T(1024)}, u32[]{:S(2)}) copy-start(f32[2048]{0:T(1024)} %param.27) | copy-start | bytes 24580
  609.8 21.0 %copy-start.9 = (f32[2048]{0:T(1024)S(1)}, f32[2048]{0:T(1024)}, u32[]{:S(2)}) copy-start(f32[2048]{0:T(1024)} %param.26) | copy-start | bytes 24580
  628.0 2.0 copy-start
Sparse Core Ops, SparseCore 0:
  9.5 95.0 all-gather.6
  106.6 91.3 all-gather.10
  200.2 90.4 all-gather.8
  300.5 18.0 all-reduce.2
  320.6 93.4 all-gather.12
  416.2 90.4 all-gather.14
  508.8 91.2 all-gather.16
  609.9 18.0 all-reduce.4
where the time goes:
time: 640 us
  waiting for transfers between devices  586 us (92%)
  matrix products  29.4 us (5%)
  between operations  13.6 us (2%)
  other arithmetic  10.4 us (2%)
    all_gather x2, waiting for transfers between devices, project_in(): lax.all_gather(gate_weight, 'fs', axis=0, tiled=True)  186 us
    all_gather x2, waiting for transfers between devices, project_out(): lax.all_gather(down_weight, 'fs', axis=1, tiled=True)  182 us
    all_gather x2, waiting for transfers between devices, project_in(): lax.all_gather(up_weight, 'fs', axis=0, tiled=True)  180 us
    psum x2, waiting for transfers between devices, half_step(): summed = lax.psum(partials.astype(jnp.bfloat16), 'tp')  34.3 us
    dot_general x2, matrix products, project_out(): jnp.dot(hidden, lax.all_gather(down_weight, 'fs', axis=1, tiled=True), pr...  19.3 us
  transfers between devices with their start and end apart: 8, of which 8 were waited for; matrix products, arithmetic and copies ran while one was open for 2% of the time, Pallas kernels for 0%

commit v1 on v0

--- a/solution.py
+++ b/solution.py
@@ -6,6 +6,18 @@
 
 residual_scale = math.sqrt(2.0)
 norm_eps = 1e-05
+
+
+def shape_the_target(mat, ax_name):
+    copies = [mat]
+    how_many = lax.axis_size(ax_name)
+    for ix in range(1, how_many):
+        left_arr = lax.ppermute(
+            copies[ix - 1], ax_name, [(num, (num - 1) % how_many) for num in range(how_many)]
+        )
+        copies.append(left_arr)
+    x_new = jnp.concatenate(copies, 0)
+    return jnp.roll(x_new, lax.axis_index(ax_name) * mat.shape[0], 0)
 
 
 def normalize(summed, scaling, offset):
@@ -20,7 +32,7 @@
 
 def project_in(inputs, gate_weight, up_weight):
     return (
-        add_columns(inputs, lax.all_gather(gate_weight, "fs", axis=0, tiled=True)),
+        add_columns(inputs, shape_the_target(gate_weight, "fs")),
         add_columns(inputs, lax.all_gather(up_weight, "fs", axis=0, tiled=True)),
     )
 

time: 640 us -> 607 us (0.948)
  waiting for transfers between devices: 586 us -> 465 us
  starting transfers between devices: 0.45 us -> 69.1 us
  local copies, waits for them, and re-layouts: 0.05 us -> 17.1 us
    ppermute x0 -> x14, waiting for transfers between devices: none -> 330 us  [shape_the_target(): lax.ppermute(copies[ix - 1], ax_name, [(num, (num - 1) % how_many) for nu...]
    all_gather x2 -> x0, waiting for transfers between devices: 186 us -> none  [project_in(): lax.all_gather(gate_weight, 'fs', axis=0, tiled=True)]
    all_gather x2, waiting for transfers between devices: 180 us -> 0.02 us  [project_in(): lax.all_gather(up_weight, 'fs', axis=0, tiled=True)]
    ppermute x0 -> x14, starting transfers between devices: none -> 68.9 us  [shape_the_target(): lax.ppermute(copies[ix - 1], ax_name, [(num, (num - 1) % how_many) for nu...]
    all_gather x2, waiting for transfers between devices: 182 us -> 115 us  [project_out(): lax.all_gather(down_weight, 'fs', axis=1, tiled=True)]
    psum x2, waiting for transfers between devices: 34.3 us -> 18.3 us  [half_step(): summed = lax.psum(partials.astype(jnp.bfloat16), 'tp')]
    unnamed x20 -> x36, local copies, waits for them, and re-layouts: 0.05 us -> 15.3 us
  transfers between devices with their start and end apart: 8 -> 20, of which waited for: 8 -> 17; matrix products, arithmetic and copies ran while one was open for 2% -> 5% of each run, Pallas kernels for 0% -> 0%
where the time goes in v1:
time: 607 us
  waiting for transfers between devices  465 us (77%)
  starting transfers between devices  69.1 us (11%)
  matrix products  31 us (5%)
  local copies, waits for them, and re-layouts  17.1 us (3%)
  between operations  13.6 us (2%)
  other arithmetic  10.4 us (2%)
    ppermute x14, waiting for transfers between devices, shape_the_target(): lax.ppermute(copies[ix - 1], ax_name, [(num, (num - 1) % how_many) for nu...  330 us
    all_gather x2, waiting for transfers between devices, project_out(): lax.all_gather(down_weight, 'fs', axis=1, tiled=True)  115 us
    ppermute x14, starting transfers between devices, shape_the_target(): lax.ppermute(copies[ix - 1], ax_name, [(num, (num - 1) % how_many) for nu...  68.9 us
    dot_general x2, matrix products, project_out(): jnp.dot(hidden, lax.all_gather(down_weight, 'fs', axis=1, tiled=True), pr...  21.4 us
    psum x2, waiting for transfers between devices, half_step(): summed = lax.psum(partials.astype(jnp.bfloat16), 'tp')  18.3 us
    unnamed x36, local copies, waits for them, and re-layouts  15.3 us
  transfers between devices with their start and end apart: 20, of which 17 were waited for; matrix products, arithmetic and copies ran while one was open for 5% of the time, Pallas kernels for 0%

profile of v1, /device:TPU:0, one launch (start us, length us, event | category | flops | bytes accessed | tf_op | source)
XLA Modules:
  0.0 606.6 jit_solution(6820558270943710014)
XLA Ops:
  6.5 0.7 all-gather.5.cloned.1.call-update
  7.3 0.7 all-gather.7.cloned.1.call-update
  8.1 6.1 %collective-permute-start = (bf16[256,1408]{1,0:T(8,128)(2,1)}, bf16[256,1408]{1,0:T(8,128)(2,1)S(1)}, u32[]{:S(2)}, u32[]{:S(2)}) collective-permute-start(bf16[256,1408]{1,0:T(8,128)(2,1)} %param.18), channel_id=1, source_target_pairs={{0,14},{2,0},{4,2},{6,4},{8,6},{10,8},{12,10},{14,12},{1,15},{3,1}... | collective-permute-start | bytes 2162696 | tf_op jit(solution)/shard_map/ppermute | solution.py:15
  14.1 25.2 %collective-permute-done = bf16[256,1408]{1,0:T(8,128)(2,1)S(1)} collective-permute-done((bf16[256,1408]{1,0:T(8,128)(2,1)}, bf16[256,1408]{1,0:T(8,128)(2,1)S(1)}, u32[]{:S(2)}, u32[]{:S(2)}) %collective-permute-start) | collective-permute-done | bytes 720928 | tf_op jit(solution)/shard_map/ppermute | solution.py:15
  39.4 5.1 collective-permute-start.1
  44.4 24.0 %collective-permute-done.1 = bf16[256,1408]{1,0:T(8,128)(2,1)S(1)} collective-permute-done((bf16[256,1408]{1,0:T(8,128)(2,1)S(1)}, bf16[256,1408]{1,0:T(8,128)(2,1)S(1)}, u32[]{:S(2)}, u32[]{:S(2)}) %collective-permute-start.1) | collective-permute-done | bytes 720928 | tf_op jit(solution)/shard_map/ppermute | solution.py:15
  68.4 5.2 collective-permute-start.2
  73.6 29.9 %collective-permute-done.2 = bf16[256,1408]{1,0:T(8,128)(2,1)S(1)} collective-permute-done((bf16[256,1408]{1,0:T(8,128)(2,1)S(1)}, bf16[256,1408]{1,0:T(8,128)(2,1)S(1)}, u32[]{:S(2)}, u32[]{:S(2)}) %collective-permute-start.2) | collective-permute-done | bytes 720928 | tf_op jit(solution)/shard_map/ppermute | solution.py:15
  103.5 5.2 collective-permute-start.3
  108.7 30.2 %collective-permute-done.3 = bf16[256,1408]{1,0:T(8,128)(2,1)S(1)} collective-permute-done((bf16[256,1408]{1,0:T(8,128)(2,1)S(1)}, bf16[256,1408]{1,0:T(8,128)(2,1)S(1)}, u32[]{:S(2)}, u32[]{:S(2)}) %collective-permute-start.3) | collective-permute-done | bytes 720928 | tf_op jit(solution)/shard_map/ppermute | solution.py:15
  138.9 5.2 collective-permute-start.4
  144.1 2.0 constant_dynamic-update-slice_fusion.7
  146.1 19.1 %collective-permute-done.4 = bf16[256,1408]{1,0:T(8,128)(2,1)} collective-permute-done((bf16[256,1408]{1,0:T(8,128)(2,1)S(1)}, bf16[256,1408]{1,0:T(8,128)(2,1)}, u32[]{:S(2)}, u32[]{:S(2)}) %collective-permute-start.4) | collective-permute-done | bytes 720928 | tf_op jit(solution)/shard_map/ppermute | solution.py:15
  165.2 5.3 collective-permute-start.5
  170.5 0.9 constant_dynamic-update-slice_fusion.6
  171.4 0.9 constant_dynamic-update-slice_fusion.5
  172.4 0.9 constant_dynamic-update-slice_fusion.4
  173.3 22.4 %collective-permute-done.5 = bf16[256,1408]{1,0:T(8,128)(2,1)S(1)} collective-permute-done((bf16[256,1408]{1,0:T(8,128)(2,1)}, bf16[256,1408]{1,0:T(8,128)(2,1)S(1)}, u32[]{:S(2)}, u32[]{:S(2)}) %collective-permute-start.5) | collective-permute-done | bytes 720928 | tf_op jit(solution)/shard_map/ppermute | solution.py:15
  195.7 5.1 collective-permute-start.6
  200.8 0.9 constant_dynamic-update-slice_fusion.3
  201.7 2.0 constant_dynamic-update-slice_fusion.2
  203.8 0.9 constant_dynamic-update-slice_fusion.1
  204.7 18.1 %collective-permute-done.6 = bf16[256,1408]{1,0:T(8,128)(2,1)S(1)} collective-permute-done((bf16[256,1408]{1,0:T(8,128)(2,1)S(1)}, bf16[256,1408]{1,0:T(8,128)(2,1)S(1)}, u32[]{:S(2)}, u32[]{:S(2)}) %collective-permute-start.6) | collective-permute-done | bytes 720928 | tf_op jit(solution)/shard_map/ppermute | solution.py:15
  222.7 0.9 constant_dynamic-update-slice_fusion
  223.7 4.8 fusion.32
  228.5 53.3 %all-gather.7.cloned.1.call-done = bf16[1408,2048]{1,0:T(8,128)(2,1)} async-done(((bf16[1408,256]{1,0:T(8,128)(2,1)}), bf16[1408,2048]{1,0:T(8,128)(2,1)}) %all-gather.7.cloned.1.call-update) | async-done | bytes 5767184 | tf_op jit(solution)/shard_map/all_gather | solution.py:43
  281.8 10.7 %convolution_convert_fusion.1 = bf16[320,2048]{1,0:T(8,128)(2,1)} fusion(bf16[1408,2048]{1,0:T(8,128)(2,1)} %all-gather.7.cloned.1.call-done, f32[320,1408]{1,0:T(8,128)S(1)} %fusion.32, bf16[320,2048]{1,0:T(8,128)(2,1)S(1)} %copy-done.2, s32[]{:T(128)S(6)} %select_n.13, bf16[2048,1408]{1,0:T(8,128)(2,1)} %constant_dynamic-update-slice_fusion), kind=kOutput, calls=%fused_computation.10 | convolution fusion | flops 3705880576 | bytes 15958020 | tf_op jit(solution)/shard_map/dot_general | solution.py:41
  292.5 0.0 all-gather.9.cloned.1.call-start
  292.6 0.5 all-gather.9.cloned.1.call-update
  293.2 0.5 all-gather.11.cloned.1.call-update
  293.7 1.5 collective-permute-start.7
  295.3 16.2 %collective-permute-done.7 = bf16[256,1408]{1,0:T(8,128)(2,1)S(1)} collective-permute-done((bf16[256,1408]{1,0:T(8,128)(2,1)S(1)}, bf16[256,1408]{1,0:T(8,128)(2,1)S(1)}, u32[]{:S(2)}, u32[]{:S(2)}) %collective-permute-start.7) | collective-permute-done | bytes 720928 | tf_op jit(solution)/shard_map/ppermute | solution.py:15
  311.5 4.4 collective-permute-start.8
  316.0 24.0 %collective-permute-done.8 = bf16[256,1408]{1,0:T(8,128)(2,1)S(1)} collective-permute-done((bf16[256,1408]{1,0:T(8,128)(2,1)S(1)}, bf16[256,1408]{1,0:T(8,128)(2,1)S(1)}, u32[]{:S(2)}, u32[]{:S(2)}) %collective-permute-start.8) | collective-permute-done | bytes 720928 | tf_op jit(solution)/shard_map/ppermute | solution.py:15
  340.0 5.2 collective-permute-start.9
  345.2 24.1 %collective-permute-done.9 = bf16[256,1408]{1,0:T(8,128)(2,1)S(1)} collective-permute-done((bf16[256,1408]{1,0:T(8,128)(2,1)S(1)}, bf16[256,1408]{1,0:T(8,128)(2,1)S(1)}, u32[]{:S(2)}, u32[]{:S(2)}) %collective-permute-start.9) | collective-permute-done | bytes 720928 | tf_op jit(solution)/shard_map/ppermute | solution.py:15
  369.2 5.2 collective-permute-start.10
  374.4 29.9 %collective-permute-done.10 = bf16[256,1408]{1,0:T(8,128)(2,1)S(1)} collective-permute-done((bf16[256,1408]{1,0:T(8,128)(2,1)S(1)}, bf16[256,1408]{1,0:T(8,128)(2,1)S(1)}, u32[]{:S(2)}, u32[]{:S(2)}) %collective-permute-start.10) | collective-permute-done | bytes 720928 | tf_op jit(solution)/shard_map/ppermute | solution.py:15
  404.3 5.2 collective-permute-start.11
  409.5 0.9 constant_dynamic-update-slice_fusion.15
  410.4 29.2 %collective-permute-done.11 = bf16[256,1408]{1,0:T(8,128)(2,1)S(1)} collective-permute-done((bf16[256,1408]{1,0:T(8,128)(2,1)S(1)}, bf16[256,1408]{1,0:T(8,128)(2,1)S(1)}, u32[]{:S(2)}, u32[]{:S(2)}) %collective-permute-start.11) | collective-permute-done | bytes 720928 | tf_op jit(solution)/shard_map/ppermute | solution.py:15
  439.7 5.2 collective-permute-start.12
  444.8 0.9 constant_dynamic-update-slice_fusion.14
  445.8 0.9 constant_dynamic-update-slice_fusion.13
  446.7 0.9 constant_dynamic-update-slice_fusion.12
  447.6 17.6 %collective-permute-done.12 = bf16[256,1408]{1,0:T(8,128)(2,1)S(1)} collective-permute-done((bf16[256,1408]{1,0:T(8,128)(2,1)S(1)}, bf16[256,1408]{1,0:T(8,128)(2,1)S(1)}, u32[]{:S(2)}, u32[]{:S(2)}) %collective-permute-start.12) | collective-permute-done | bytes 720928 | tf_op jit(solution)/shard_map/ppermute | solution.py:15
  465.2 5.2 collective-permute-start.13
  470.4 0.9 constant_dynamic-update-slice_fusion.11
  471.3 0.9 constant_dynamic-update-slice_fusion.10
  472.3 0.9 constant_dynamic-update-slice_fusion.9
  473.2 19.9 %collective-permute-done.13 = bf16[256,1408]{1,0:T(8,128)(2,1)S(1)} collective-permute-done((bf16[256,1408]{1,0:T(8,128)(2,1)S(1)}, bf16[256,1408]{1,0:T(8,128)(2,1)S(1)}, u32[]{:S(2)}, u32[]{:S(2)}) %collective-permute-start.13) | collective-permute-done | bytes 720928 | tf_op jit(solution)/shard_map/ppermute | solution.py:15
  493.1 0.9 constant_dynamic-update-slice_fusion.8
  494.0 2.1 fusion.14
  496.1 0.8 multiply_reduce_fusion.2
  496.9 1.3 fusion.9
  498.3 0.7 multiply_reduce_fusion.1
  499.0 0.8 add_convert_fusion.1
  499.8 4.8 fusion.33
  504.6 61.3 %all-gather.11.cloned.1.call-done = bf16[1408,2048]{1,0:T(8,128)(2,1)} async-done(((bf16[1408,256]{1,0:T(8,128)(2,1)}), bf16[1408,2048]{1,0:T(8,128)(2,1)}) %all-gather.11.cloned.1.call-update) | async-done | bytes 5767184 | tf_op jit(solution)/shard_map/all_gather | solution.py:43
  566.0 10.7 %convolution_convert_fusion = bf16[320,2048]{1,0:T(8,128)(2,1)} fusion(bf16[1408,2048]{1,0:T(8,128)(2,1)} %all-gather.11.cloned.1.call-done, f32[320,1408]{1,0:T(8,128)S(1)} %fusion.33, bf16[320,2048]{1,0:T(8,128)(2,1)S(1)} %add_convert_fusion.1, s32[]{:T(128)S(6)} %select_n.13, bf16[2048,1408]{1,0:T(8,128)(2,1)} %constant_dynamic-update-slice_fusion.8), kind=kOutput, calls=%fused_computation.9 | convolution fusion | flops 3705880576 | bytes 15958020 | tf_op jit(solution)/shard_map/dot_general | solution.py:41
  576.7 18.3 %all-reduce.5.cloned.1.call-done = bf16[320,2048]{1,0:T(8,128)(2,1)} async-done(((bf16[320,2048]{1,0:T(8,128)(2,1)}), bf16[320,2048]{1,0:T(8,128)(2,1)}) %all-reduce.5.cloned.1.call-update) | async-done | bytes 1310736 | tf_op jit(solution)/shard_map/psum | solution.py:52
  595.0 2.0 fusion.15
  597.0 0.8 multiply_reduce_fusion
  597.8 1.9 add_convert_fusion
  (38 shorter events, 0.3 us)
Async XLA Ops:
  6.5 217.1 %all-gather.5.cloned.1.call-start = ((), (), s32[]{:S(2)}) async-start(), calls=%async_computation | async-start | bytes 6488064 | tf_op jit(solution)/shard_map/all_gather | solution.py:36
  7.3 274.6 %all-gather.7.cloned.1.call-start = ((), (), s32[]{:S(2)}) async-start(), calls=%async_computation.1 | async-start | bytes 6488064 | tf_op jit(solution)/shard_map/all_gather | solution.py:43
  8.0 486.0 %all-reduce.3.cloned.1.call-start = ((), (), s32[]{:S(2)}) async-start(), calls=%async_computation.2 | async-start | bytes 2621440 | tf_op jit(solution)/shard_map/psum | solution.py:52
  8.1 31.3 %collective-permute-start = (bf16[256,1408]{1,0:T(8,128)(2,1)}, bf16[256,1408]{1,0:T(8,128)(2,1)S(1)}, u32[]{:S(2)}, u32[]{:S(2)}) collective-permute-start(bf16[256,1408]{1,0:T(8,128)(2,1)} %param.18), channel_id=1, source_target_pairs={{0,14},{2,0},{4,2},{6,4},{8,6},{10,8},{12,10},{14,12},{1,15},{3,1}... | collective-permute-start | bytes 2162696 | tf_op jit(solution)/shard_map/ppermute | solution.py:15
  39.4 29.0 %collective-permute-start.1 = (bf16[256,1408]{1,0:T(8,128)(2,1)S(1)}, bf16[256,1408]{1,0:T(8,128)(2,1)S(1)}, u32[]{:S(2)}, u32[]{:S(2)}) collective-permute-start(bf16[256,1408]{1,0:T(8,128)(2,1)S(1)} %collective-permute-done), channel_id=1, source_target_pairs={{0,14},{2,0},{4,2},{6,4},{8,6},{10,8},{12,10},{14,12},{1,15},{3,1}... | collective-permute-start | bytes 2162696 | tf_op jit(solution)/shard_map/ppermute | solution.py:15
  68.4 35.1 %collective-permute-start.2 = (bf16[256,1408]{1,0:T(8,128)(2,1)S(1)}, bf16[256,1408]{1,0:T(8,128)(2,1)S(1)}, u32[]{:S(2)}, u32[]{:S(2)}) collective-permute-start(bf16[256,1408]{1,0:T(8,128)(2,1)S(1)} %collective-permute-done.1), channel_id=1, source_target_pairs={{0,14},{2,0},{4,2},{6,4},{8,6},{10,8},{12,10},{14,12},{1,15},{3,1}... | collective-permute-start | bytes 2162696 | tf_op jit(solution)/shard_map/ppermute | solution.py:15
  103.5 35.4 %collective-permute-start.3 = (bf16[256,1408]{1,0:T(8,128)(2,1)S(1)}, bf16[256,1408]{1,0:T(8,128)(2,1)S(1)}, u32[]{:S(2)}, u32[]{:S(2)}) collective-permute-start(bf16[256,1408]{1,0:T(8,128)(2,1)S(1)} %collective-permute-done.2), channel_id=1, source_target_pairs={{0,14},{2,0},{4,2},{6,4},{8,6},{10,8},{12,10},{14,12},{1,15},{3,1}... | collective-permute-start | bytes 2162696 | tf_op jit(solution)/shard_map/ppermute | solution.py:15
  138.9 26.3 %collective-permute-start.4 = (bf16[256,1408]{1,0:T(8,128)(2,1)S(1)}, bf16[256,1408]{1,0:T(8,128)(2,1)}, u32[]{:S(2)}, u32[]{:S(2)}) collective-permute-start(bf16[256,1408]{1,0:T(8,128)(2,1)S(1)} %collective-permute-done.3), channel_id=1, source_target_pairs={{0,14},{2,0},{4,2},{6,4},{8,6},{10,8},{12,10},{14,12},{1,15},{3,1}... | collective-permute-start | bytes 2162696 | tf_op jit(solution)/shard_map/ppermute | solution.py:15
  165.2 30.5 %collective-permute-start.5 = (bf16[256,1408]{1,0:T(8,128)(2,1)}, bf16[256,1408]{1,0:T(8,128)(2,1)S(1)}, u32[]{:S(2)}, u32[]{:S(2)}) collective-permute-start(bf16[256,1408]{1,0:T(8,128)(2,1)} %collective-permute-done.4), channel_id=1, source_target_pairs={{0,14},{2,0},{4,2},{6,4},{8,6},{10,8},{12,10},{14,12},{1,15},{3,1}... | collective-permute-start | bytes 2162696 | tf_op jit(solution)/shard_map/ppermute | solution.py:15
  173.3 50.4 %copy-start.2 = (bf16[320,2048]{1,0:T(8,128)(2,1)S(1)}, bf16[320,2048]{1,0:T(8,128)(2,1)}, u32[]{:S(2)}) copy-start(bf16[320,2048]{1,0:T(8,128)(2,1)} %param.16) | copy-start | bytes 3932164
  195.7 27.0 %collective-permute-start.6 = (bf16[256,1408]{1,0:T(8,128)(2,1)S(1)}, bf16[256,1408]{1,0:T(8,128)(2,1)S(1)}, u32[]{:S(2)}, u32[]{:S(2)}) collective-permute-start(bf16[256,1408]{1,0:T(8,128)(2,1)S(1)} %collective-permute-done.5), channel_id=1, source_target_pairs={{0,14},{2,0},{4,2},{6,4},{8,6},{10,8},{12,10},{14,12},{1,15},{3,1}... | collective-permute-start | bytes 2162696 | tf_op jit(solution)/shard_map/ppermute | solution.py:15
  292.5 1.2 copy-start.4
  292.5 207.3 %all-gather.9.cloned.1.call-start = ((), (), s32[]{:S(2)}) async-start(), calls=%async_computation.3 | async-start | bytes 6488064 | tf_op jit(solution)/shard_map/all_gather | solution.py:36
  293.1 272.9 %all-gather.11.cloned.1.call-start = ((), (), s32[]{:S(2)}) async-start(), calls=%async_computation.4 | async-start | bytes 6488064 | tf_op jit(solution)/shard_map/all_gather | solution.py:43
  293.7 301.3 %all-reduce.5.cloned.1.call-start = ((), (), s32[]{:S(2)}) async-start(), calls=%async_computation.5 | async-start | bytes 2621440 | tf_op jit(solution)/shard_map/psum | solution.py:52
  293.7 17.8 %collective-permute-start.7 = (bf16[256,1408]{1,0:T(8,128)(2,1)S(1)}, bf16[256,1408]{1,0:T(8,128)(2,1)S(1)}, u32[]{:S(2)}, u32[]{:S(2)}) collective-permute-start(bf16[256,1408]{1,0:T(8,128)(2,1)S(1)} %copy-done.4), channel_id=1, source_target_pairs={{0,14},{2,0},{4,2},{6,4},{8,6},{10,8},{12,10},{14,12},{1,15},{3,1}... | collective-permute-start | bytes 2162696 | tf_op jit(solution)/shard_map/ppermute | solution.py:15
  311.5 28.5 %collective-permute-start.8 = (bf16[256,1408]{1,0:T(8,128)(2,1)S(1)}, bf16[256,1408]{1,0:T(8,128)(2,1)S(1)}, u32[]{:S(2)}, u32[]{:S(2)}) collective-permute-start(bf16[256,1408]{1,0:T(8,128)(2,1)S(1)} %collective-permute-done.7), channel_id=1, source_target_pairs={{0,14},{2,0},{4,2},{6,4},{8,6},{10,8},{12,10},{14,12},{1,15},{3,1}... | collective-permute-start | bytes 2162696 | tf_op jit(solution)/shard_map/ppermute | solution.py:15
  340.0 29.2 %collective-permute-start.9 = (bf16[256,1408]{1,0:T(8,128)(2,1)S(1)}, bf16[256,1408]{1,0:T(8,128)(2,1)S(1)}, u32[]{:S(2)}, u32[]{:S(2)}) collective-permute-start(bf16[256,1408]{1,0:T(8,128)(2,1)S(1)} %collective-permute-done.8), channel_id=1, source_target_pairs={{0,14},{2,0},{4,2},{6,4},{8,6},{10,8},{12,10},{14,12},{1,15},{3,1}... | collective-permute-start | bytes 2162696 | tf_op jit(solution)/shard_map/ppermute | solution.py:15
  369.2 35.1 %collective-permute-start.10 = (bf16[256,1408]{1,0:T(8,128)(2,1)S(1)}, bf16[256,1408]{1,0:T(8,128)(2,1)S(1)}, u32[]{:S(2)}, u32[]{:S(2)}) collective-permute-start(bf16[256,1408]{1,0:T(8,128)(2,1)S(1)} %collective-permute-done.9), channel_id=1, source_target_pairs={{0,14},{2,0},{4,2},{6,4},{8,6},{10,8},{12,10},{14,12},{1,15},{3,1}... | collective-permute-start | bytes 2162696 | tf_op jit(solution)/shard_map/ppermute | solution.py:15
  404.3 35.4 %collective-permute-start.11 = (bf16[256,1408]{1,0:T(8,128)(2,1)S(1)}, bf16[256,1408]{1,0:T(8,128)(2,1)S(1)}, u32[]{:S(2)}, u32[]{:S(2)}) collective-permute-start(bf16[256,1408]{1,0:T(8,128)(2,1)S(1)} %collective-permute-done.10), channel_id=1, source_target_pairs={{0,14},{2,0},{4,2},{6,4},{8,6},{10,8},{12,10},{14,12},{1,15},{3,1}... | collective-permute-start | bytes 2162696 | tf_op jit(solution)/shard_map/ppermute | solution.py:15
  439.7 25.6 %collective-permute-start.12 = (bf16[256,1408]{1,0:T(8,128)(2,1)S(1)}, bf16[256,1408]{1,0:T(8,128)(2,1)S(1)}, u32[]{:S(2)}, u32[]{:S(2)}) collective-permute-start(bf16[256,1408]{1,0:T(8,128)(2,1)S(1)} %collective-permute-done.11), channel_id=1, source_target_pairs={{0,14},{2,0},{4,2},{6,4},{8,6},{10,8},{12,10},{14,12},{1,15},{3,1}... | collective-permute-start | bytes 2162696 | tf_op jit(solution)/shard_map/ppermute | solution.py:15
  465.2 27.9 %collective-permute-start.13 = (bf16[256,1408]{1,0:T(8,128)(2,1)S(1)}, bf16[256,1408]{1,0:T(8,128)(2,1)S(1)}, u32[]{:S(2)}, u32[]{:S(2)}) collective-permute-start(bf16[256,1408]{1,0:T(8,128)(2,1)S(1)} %collective-permute-done.12), channel_id=1, source_target_pairs={{0,14},{2,0},{4,2},{6,4},{8,6},{10,8},{12,10},{14,12},{1,15},{3,1}... | collective-permute-start | bytes 2162696 | tf_op jit(solution)/shard_map/ppermute | solution.py:15
  494.0 2.9 copy-start.1
  494.0 2.1 copy-start.3
  494.0 2.9 copy-start.5
  494.0 2.9 copy-start.6
  498.2 0.7 copy-start.7
  498.2 0.7 copy-start.8
  576.7 21.1 %copy-start.9 = (f32[2048]{0:T(1024)S(1)}, f32[2048]{0:T(1024)}, u32[]{:S(2)}) copy-start(f32[2048]{0:T(1024)} %param.29) | copy-start | bytes 24580
  576.7 21.1 %copy-start.10 = (f32[2048]{0:T(1024)S(1)}, f32[2048]{0:T(1024)}, u32[]{:S(2)}) copy-start(f32[2048]{0:T(1024)} %param.28) | copy-start | bytes 24580
  595.0 2.0 copy-start
Sparse Core Ops, SparseCore 0:
  9.5 149.5 all-gather.4
  161.1 120.6 all-gather.6
  292.6 18.1 all-reduce.2
  312.9 147.1 all-gather.8
  462.0 103.9 all-gather.10
  576.8 18.1 all-reduce.4
